TPU v7x, 32 devices: a whole 2x2x4 slice. The times are simulated.
32 devices in a mesh: sp: 4 (over z), tp: 4 (over y, x), dp: 2 (over core).
Axes of the slice: x: 2, y: 2, z: 4, core: 2. Of those that a mesh axis runs over, the one named last changes fastest.
Arguments:
- latent: bfloat16 [2048, 4, 2048], P(('sp', 'tp'), 'dp'), may hold values from -6 to 6
- context: bfloat16 [1024, 4, 2048], P('sp', 'dp'), may hold values from -6 to 6
- condition: bfloat16 [4, 2048], P('dp', 'sp'), may hold values from -6 to 6
- ctx_condition: bfloat16 [2048], P('sp'), may hold values from -6 to 6
- norm_gain: float32 [2048], replicated, may hold values from 0.1 to 1.9
- w_shift: bfloat16 [2048, 2048], P('sp', 'tp'), may hold values from -0.1875 to 0.1875
- w_scale: bfloat16 [2048, 2048], P('sp', 'tp'), may hold values from -0.1875 to 0.1875
- w_gate: bfloat16 [2048, 2048], P('sp', 'tp'), may hold values from -0.1875 to 0.1875
- w_query: bfloat16 [2048, 2048], P(None, 'tp'), may hold values from -0.125 to 0.125
- w_key: bfloat16 [2048, 512], P(None, 'tp'), may hold values from -6 to 6
- w_value: bfloat16 [2048, 512], P(None, 'tp'), may hold values from -0.125 to 0.125
- w_out: bfloat16 [2048, 2048], P('tp'), may hold values from -1 to 1
- sink: float32 [16], P('tp'), may hold values from 5 to 9
Outputs:
- mixed: bfloat16 [2048, 4, 2048], P(('sp', 'tp'), 'dp')
All inputs are finite; a program needn't handle non-finite values.
Results may differ from a plain program's by a relative error of at most 0.015.
The roundings to bfloat16 on the way count: a program that leaves them out, or rounds other values in their place, can miss the bound.
Values may be sent and summed in bfloat16 or wider, within the bound.
A program may use at most 128 MiB of HBM per device.

v0:
```python
import jax
import jax.numpy as jnp
from jax import lax
from jax.sharding import PartitionSpec as P

HEAD_DIM = 128
WINDOW = 128
GRID_W = 64


EPSILON = 1e-06
NEGATIVE = -1e30


def padded_2(shard, sides, width):
    for axis, dim in sides:
        size, length = (lax.axis_size(axis), shard.shape[dim])
        up = [(i, (i + 1) % size) for i in range(size - 1)]
        down = [(j, i) for i, j in up]
        last = lax.slice_in_dim(shard, length - width, length, axis=dim)
        leading = lax.slice_in_dim(shard, 0, width, axis=dim)
        before = lax.ppermute(last, axis, up)
        after = lax.ppermute(leading, axis, down)
        shard = jnp.concatenate([before, shard, after], axis=dim)
    return shard


def normed(values, gain):
    floats = values.astype(jnp.float32)
    return floats * lax.rsqrt(jnp.mean(floats * floats, axis=-1, keepdims=True) + EPSILON) * gain


def rotate(tensor, position):
    quarter = HEAD_DIM // 4
    freqs = 10000.0 ** (-jnp.arange(quarter, dtype=jnp.float32) / quarter)
    row_pos = (position // GRID_W).astype(jnp.float32)
    col_pos = (position % GRID_W).astype(jnp.float32)
    angle = jnp.stack([row_pos[:, None] * freqs, col_pos[:, None] * freqs], axis=1)
    cosine = jnp.cos(angle)[:, None, None]
    sine = jnp.sin(angle)[:, None, None]
    pieces = tensor.reshape(tensor.shape[:-1] + (2, 2, quarter))
    first = pieces[..., 0, :]
    second = pieces[..., 1, :]
    turned = jnp.stack([first * cosine - second * sine, second * cosine + first * sine], axis=-2)
    return turned.reshape(tensor.shape)


def local(
    latent,
    context,
    condition,
    ctx_condition,
    norm_gain,
    w_shift,
    w_scale,
    w_gate,
    w_query,
    w_key,
    w_value,
    w_out,
    sink,
):
    samples_n = latent.shape[1]
    act = jax.nn.silu(condition.astype(jnp.float32)).astype(jnp.bfloat16)
    ctx_act = jax.nn.silu(ctx_condition.astype(jnp.float32)).astype(jnp.bfloat16)
    both = jnp.concatenate([act, ctx_act[None]], axis=0)
    pair_part = jnp.stack(
        [
            jnp.dot(both, w_shift, preferred_element_type=jnp.float32),
            jnp.dot(both, w_scale, preferred_element_type=jnp.float32),
        ]
    )
    gate_part = jnp.dot(act, w_gate, preferred_element_type=jnp.float32)
    pair_sum, gate_sum = lax.psum((pair_part, gate_part), "sp")
    pair_full, gate = (
        lax.all_gather(pair_sum, "tp", axis=2, tiled=True),
        lax.all_gather(gate_sum, "tp", axis=1, tiled=True),
    )
    hidden = (
        normed(latent, norm_gain) * (1.0 + pair_full[1, :samples_n][None])
        + pair_full[0, :samples_n][None]
    ).astype(jnp.bfloat16)
    ctx_hidden = (
        normed(context, norm_gain) * (1.0 + pair_full[1, samples_n]) + pair_full[0, samples_n]
    ).astype(jnp.bfloat16)
    block_len = latent.shape[0] * lax.axis_size("tp")
    block_start = lax.axis_index("sp") * block_len
    seq_total = block_len * lax.axis_size("sp")
    q_width = w_query.shape[1]
    k_width = w_key.shape[1]
    local_heads = q_width // HEAD_DIM
    local_kv = k_width // HEAD_DIM
    w_project = jnp.concatenate([w_query, w_key, w_value], axis=1)
    piece = lax.all_gather(hidden, "tp", axis=0, tiled=True)
    count = piece.shape[0]
    product = jnp.dot(piece, w_project, preferred_element_type=jnp.float32)
    position = block_start + jnp.arange(count, dtype=jnp.int32)
    rot_q = rotate(
        product[..., :q_width].reshape(count, samples_n, local_heads, HEAD_DIM), position
    )
    rot_k = rotate(
        product[..., q_width : q_width + k_width].reshape(count, samples_n, local_kv, HEAD_DIM),
        position,
    )
    projected = jnp.concatenate(
        [
            rot_q.reshape(count, samples_n, q_width),
            rot_k.reshape(count, samples_n, k_width),
            product[..., q_width + k_width :],
        ],
        axis=-1,
    ).astype(jnp.bfloat16)
    queries = projected[..., :q_width]
    padded = padded_2(projected[..., q_width:], (("sp", 0),), WINDOW)
    w_pair = jnp.concatenate([w_key, w_value], axis=1)
    local_pair = jnp.dot(ctx_hidden, w_pair, preferred_element_type=jnp.float32).astype(
        jnp.bfloat16
    )
    ctx_pair = lax.all_gather(local_pair, "sp", axis=0, tiled=True)
    span = padded.shape[0]
    ctx_len = ctx_pair.shape[0]
    group = local_heads // local_kv
    grouped = queries.reshape(block_len, samples_n, local_kv, group, HEAD_DIM)
    keys = padded[..., :k_width].reshape(span, samples_n, local_kv, HEAD_DIM)
    values = padded[..., k_width:].reshape(span, samples_n, local_kv, HEAD_DIM)
    ctx_keys = ctx_pair[..., :k_width].reshape(ctx_len, samples_n, local_kv, HEAD_DIM)
    ctx_values = ctx_pair[..., k_width:].reshape(ctx_len, samples_n, local_kv, HEAD_DIM)
    factor = HEAD_DIM ** (-0.5)
    q_index = jnp.arange(block_len, dtype=jnp.int32)
    k_index = jnp.arange(span, dtype=jnp.int32)
    k_global = block_start - WINDOW + k_index
    allowed = (
        (jnp.abs((k_index - WINDOW)[None, :] - q_index[:, None]) <= WINDOW)
        & (k_global >= 0)[None, :]
        & (k_global < seq_total)[None, :]
    )
    local_scores = (
        jnp.einsum("qbkgd,jbkd->bkgqj", grouped, keys, preferred_element_type=jnp.float32) * factor
    )
    local_scores = jnp.where(allowed, local_scores, NEGATIVE)
    ctx_scores = (
        jnp.einsum("qbkgd,jbkd->bkgqj", grouped, ctx_keys, preferred_element_type=jnp.float32)
        * factor
    )
    sink_scores = sink.reshape(local_kv, group)[None, :, :, None, None]
    top = jnp.maximum(
        jnp.maximum(
            jnp.max(local_scores, axis=-1, keepdims=True),
            jnp.max(ctx_scores, axis=-1, keepdims=True),
        ),
        sink_scores,
    )
    local_exp = jnp.exp(local_scores - top)
    ctx_exp = jnp.exp(ctx_scores - top)
    total = (
        jnp.sum(local_exp, axis=-1, keepdims=True)
        + jnp.sum(ctx_exp, axis=-1, keepdims=True)
        + jnp.exp(sink_scores - top)
    )
    local_weights = (local_exp / total).astype(jnp.bfloat16)
    ctx_weights = (ctx_exp / total).astype(jnp.bfloat16)
    attn = jnp.einsum(
        "bkgqj,jbkd->qbkgd", local_weights, values, preferred_element_type=jnp.float32
    )
    attn = attn + jnp.einsum(
        "bkgqj,jbkd->qbkgd", ctx_weights, ctx_values, preferred_element_type=jnp.float32
    )
    attn = attn.astype(jnp.bfloat16).reshape(block_len, samples_n, q_width)
    branch = lax.psum_scatter(
        jnp.dot(attn, w_out, preferred_element_type=jnp.float32).astype(jnp.bfloat16),
        "tp",
        scatter_dimension=0,
        tiled=True,
    ).astype(jnp.float32)
    return (latent.astype(jnp.float32) + gate[None] * branch).astype(jnp.bfloat16)


def solution(mesh):
    return jax.shard_map(
        local,
        mesh=mesh,
        in_specs=(
            P(("sp", "tp"), "dp", None),
            P("sp", "dp", None),
            P("dp", "sp"),
            P("sp"),
            P(),
            P("sp", "tp"),
            P("sp", "tp"),
            P("sp", "tp"),
            P(None, "tp"),
            P(None, "tp"),
            P(None, "tp"),
            P("tp", None),
            P("tp"),
        ),
        out_specs=P(("sp", "tp"), "dp", None),
        check_vma=False,
    )
```

profile of v0, /device:TPU:0, one launch (start us, length us, event | category | flops | bytes accessed | tf_op | source)
XLA Modules:
  0.0 239.7 jit_solution(1467744613596993384)
XLA Ops:
  6.5 0.0 copy-start
  6.5 0.8 fusion.49
  7.4 0.7 fusion.44
  8.1 0.0 copy-start.7
  8.1 1.2 convolution_bitcast_fusion
  9.3 1.2 convolution_bitcast_fusion.1
  10.5 1.2 fusion.62
  11.8 20.7 %all-reduce = (f32[2,3,512]{2,1,0:T(4,128)S(1)}, f32[2,512]{1,0:T(2,128)S(1)}) all-reduce(f32[2,3,512]{2,1,0:T(4,128)S(1)} %pad_maximum_fusion.6, f32[2,512]{1,0:T(2,128)S(1)} %fusion.62), channel_id=1, replica_groups=mesh['sp'=4,'tp'=4,'dp'=2] {'sp'}, use_global_device_ids=true, to_apply=%region_2.3 | all-reduce | flops 4096 | bytes 32768 | tf_op jit(solution)/shard_map/psum | solution.py:74
  32.5 8.2 %all_gather.13 = f32[2,3,2048]{2,1,0:T(4,128)S(1)} all-gather(f32[2,3,512]{2,1,0:T(4,128)S(1)} %get-tuple-element.5), channel_id=1, replica_groups=mesh['sp'=4,'tp'=4,'dp'=2] {'tp'}, dimensions={2}, use_global_device_ids=true | all-gather | bytes 61440 | tf_op jit(solution)/shard_map/all_gather | solution.py:76
  40.7 1.6 fusion.19
  42.4 2.8 %fusion.23 = bf16[128,2,2048]{2,0,1:T(8,128)(2,1)} fusion(f32[2,2048]{1,0:T(2,128)S(1)} %get-tuple-element.18, f32[2,2048]{1,0:T(2,128)S(1)} %get-tuple-element.17, f32[2048]{0:T(1024)} %param.17, f32[128,2]{0,1:T(2,128)S(1)} %add_rsqrt_fusion.1, bf16[128,2,2048]{2,1,0:T(2,128)(2,1)} %param.13), kind=kLoop, calls=%fused_computation.36 | loop fusion | flops 3145728 | bytes 2139136 | tf_op jit(solution)/shard_map/convert_element_type | solution.py:82
  45.2 0.0 all-gather.3.cloned.1.call-update
  45.2 0.0 all-gather.5.cloned.1.call-start
  45.3 3.9 %fusion.9 = f32[256,2]{1,0:T(8,128)S(1)} fusion(bf16[256,2,2048]{2,1,0:T(2,128)(2,1)} %param.14), kind=kLoop, calls=%fused_computation.17 | loop fusion | flops 3145216 | bytes 2099200 | tf_op jit(solution)/shard_map/reduce_sum | solution.py:30
  49.3 5.1 %fusion.13 = bf16[256,2,2048]{2,1,0:T(2,128)(2,1)S(1)} fusion(bf16[256,2,2048]{2,1,0:T(2,128)(2,1)} %param.14, f32[2048]{0:T(1024)S(1)} %bitcast.104, f32[2048]{0:T(1024)S(1)} %bitcast.103, f32[2048]{0:T(1024)S(1)} %copy-done.7, f32[256,2]{1,0:T(8,128)S(1)} %add_rsqrt_fusion), kind=kLoop, calls=%fused_computation.21 | loop fusion | flops 6291456 | bytes 4220928 | tf_op jit(solution)/shard_map/convert_element_type | solution.py:85
  54.3 0.0 copy-done.9
  54.3 0.0 copy-done.10
  54.3 2.1 fusion.32
  56.4 0.0 all-gather.5.cloned.1.call-update
  56.4 0.0 reduce-scatter.2.cloned.1.call-start
  56.6 0.1 broadcast_multiply_fusion.1
  56.6 0.5 fusion.40
  57.1 0.8 fusion.29
  57.9 37.4 %all-gather.3.cloned.1.call-done = bf16[512,2,2048]{2,0,1:T(8,128)(2,1)} async-done(((bf16[128,2,2048]{2,0,1:T(8,128)(2,1)}), bf16[512,2,2048]{2,0,1:T(8,128)(2,1)}) %all-gather.3.cloned.1.call-update) | async-done | bytes 4194320 | tf_op jit(solution)/shard_map/all_gather | solution.py:94
  95.3 6.4 %fusion.14 = f32[512,2,768]{2,0,1:T(8,128)S(1)} fusion(bf16[512,2,2048]{2,0,1:T(8,128)(2,1)} %all-gather.3.cloned.1.call-done, bf16[2048,128]{1,0:T(8,128)(2,1)S(1)} %copy-done.9, bf16[2048,128]{1,0:T(8,128)(2,1)} %param.22, bf16[2048,512]{1,0:T(8,128)(2,1)} %param.21), kind=kOutput, calls=%fused_computation.24 | convolution fusion | flops 3230662656 | bytes 10485760 | tf_op jit(solution)/shard_map/dot_general | solution.py:96
  101.7 0.8 slice.78
  102.6 1.6 slice.84
  104.2 1.2 copy.51
  105.4 0.1 subtract_convert_fusion.1
  105.6 0.2 copy.52
  105.7 0.0 copy-start.4
  105.7 0.8 pad_maximum_fusion.4
  106.5 4.0 %collective-permute-start = (bf16[128,2,256]{2,0,1:T(8,128)(2,1)}, bf16[128,2,256]{2,0,1:T(8,128)(2,1)}, u32[]{:S(2)}, u32[]{:S(2)}) collective-permute-start(bf16[128,2,256]{2,0,1:T(8,128)(2,1)} %get-tuple-element.11), channel_id=1, source_target_pairs={{0,8},{8,16},{16,24},{1,9},{9,17},{17,25},{2,10},{10,18},{18,26},{... | collective-permute-start | bytes 393224 | tf_op jit(solution)/shard_map/ppermute | solution.py:22
  110.6 1.5 collective-permute-start.1
  112.1 2.9 %copy.53 = f32[512,2,512]{0,2,1:T(8,128)} copy(f32[512,2,512]{2,0,1:T(8,128)} %slice.84) | data formatting | bytes 4194304 | tf_op jit(solution)/shard_map/slice | solution.py:99
  115.0 1.9 subtract_convert_fusion
  116.9 0.1 pad_maximum_fusion
  117.0 10.6 %all-gather.5.cloned.1.call-done = bf16[1024,2,256]{2,0,1:T(8,128)(2,1)} async-done(((bf16[256,2,256]{2,0,1:T(8,128)(2,1)}), bf16[1024,2,256]{2,0,1:T(8,128)(2,1)}) %all-gather.5.cloned.1.call-update) | async-done | bytes 1048592 | tf_op jit(solution)/shard_map/all_gather | solution.py:119
  127.6 9.2 %bitcast_reduce_fusion = (f32[2,4,512]{2,1,0:T(4,128)S(1)}, f32[2,1024,512,4]{2,1,3,0:T(8,128)}) fusion(bf16[512,2,4,128]{0,3,2,1:T(8,128)(2,1)S(1)} %bitcast.98, bf16[1024,2,256]{2,0,1:T(8,128)(2,1)} %all-gather.5.cloned.1.call-done), kind=kOutput, calls=%fused_computation.1 | convolution fusion | flops 1082126336 | bytes 18366464 | tf_op jit(solution)/shard_map/qbkgd,jbkd->bkgqj/dot_general | solution.py:142
  136.8 0.0 collective-permute-done
  136.8 0.0 collective-permute-done.1
  136.8 0.0 copy-done.3
  136.8 0.0 copy-done.5
  136.8 1.1 pad_maximum_fusion.1
  137.9 0.0 copy-start.8
  137.9 6.8 %fusion.3 = (f32[2,4,512]{2,1,0:T(4,128)S(1)}, f32[2,768,512,4]{2,1,3,0:T(8,128)}) fusion(pred[512,768]{0,1:T(8,128)(4,1)S(1)} %fusion.29, bf16[512,2,4,128]{0,3,2,1:T(8,128)(2,1)S(1)} %bitcast.99, bf16[768,2,256]{2,0,1:T(8,128)(2,1)S(1)} %pad_maximum_fusion.1), kind=kOutput, calls=%fused_computation.9 | convolution fusion | flops 814739456 | bytes 14434304 | tf_op jit(solution)/shard_map/qbkgd,jbkd->bkgqj/dot_general | solution.py:138
  144.7 0.1 maximum_maximum_fusion
  144.7 8.5 %fusion.1 = f32[2,4,512]{2,1,0:T(4,128)S(1)} fusion(f32[2,1024,512,4]{2,1,3,0:T(8,128)} %get-tuple-element.24, f32[2,4,512]{2,1,0:T(4,128)S(1)} %maximum_maximum_fusion), kind=kLoop, calls=%fused_computation.4 | loop fusion | flops 12578816 | bytes 16809984 | tf_op jit(solution)/shard_map/reduce_sum | solution.py:157
  153.3 0.0 slice-start
  153.3 7.3 %fusion.2 = f32[2,4,512]{2,1,0:T(4,128)S(1)} fusion(f32[2,768,512,4]{2,1,3,0:T(8,128)} %get-tuple-element.22, f32[2,4,512]{2,1,0:T(4,128)S(1)} %maximum_maximum_fusion, pred[512,768]{0,1:T(8,128)(4,1)S(1)} %fusion.29), kind=kLoop, calls=%fused_computation.8 | loop fusion | flops 12578816 | bytes 13008896 | tf_op jit(solution)/shard_map/reduce_sum | solution.py:156
  160.6 0.1 exponential_add_fusion
  160.7 0.0 copy-done.6
  160.7 0.0 slice-start.1
  160.7 0.0 slice-start.2
  160.7 8.1 %fusion.4 = f32[2,128,4,512]{3,1,2,0:T(8,128)S(1)} fusion(f32[2,1024,512,4]{2,1,3,0:T(8,128)} %get-tuple-element.24, f32[2,4,512]{2,1,0:T(4,128)S(1)} %exponential_add_fusion, f32[2,4,512]{2,1,0:T(4,128)S(1)} %maximum_maximum_fusion, bf16[1024,2,256]{2,0,1:T(8,128)(2,1)S(1)} %copy-done.6), kind=kOutput, calls=%fused_computation.10 | convolution fusion | flops 1090519040 | bytes 19431424 | tf_op jit(solution)/shard_map/bkgqj,jbkd->qbkgd/dot_general | solution.py:165
  168.9 0.1 slice-done.2
  169.0 3.8 %add_convert_fusion = bf16[2,128,4,512]{3,1,2,0:T(8,128)(2,1)S(1)} fusion(f32[2,128,4,512]{3,1,2,0:T(8,128)S(1)} %fusion.4, f32[2,4,512]{2,1,0:T(4,128)S(1)} %exponential_add_fusion, f32[2,4,512]{2,1,0:T(4,128)S(1)} %maximum_maximum_fusion, f32[2,768,512,4]{2,1,3,0:T(8,128)S(1)} %bitcast.97, pred[512,768]{0,1:T(8,128)(4,1)S(1)} %fusion.29, ...), kind=kOutput, calls=%fused_computation.41 | convolution fusion | flops 822083584 | bytes 16547840 | tf_op jit(solution)/shard_map/bkgqj,jbkd->qbkgd/dot_general | solution.py:162
  172.8 0.0 copy-done
  172.8 4.3 %convolution_convert_fusion = bf16[512,2,2048]{2,0,1:T(8,128)(2,1)} fusion(bf16[512,2,512]{0,2,1:T(8,128)(2,1)S(1)} %bitcast.105, bf16[512,2048]{1,0:T(8,128)(2,1)S(1)} %copy-done), kind=kOutput, calls=%fused_computation.22 | convolution fusion | flops 2149580800 | bytes 7340032 | tf_op jit(solution)/shard_map/dot_general | solution.py:170
  177.2 0.0 reduce-scatter.2.cloned.1.call-update
  177.2 8.3 %all_gather.12 = f32[2,2048]{1,0:T(2,128)S(1)} all-gather(f32[2,512]{1,0:T(2,128)S(1)} %get-tuple-element.6), channel_id=1, replica_groups=mesh['sp'=4,'tp'=4,'dp'=2] {'tp'}, dimensions={1}, use_global_device_ids=true | all-gather | bytes 20480 | tf_op jit(solution)/shard_map/all_gather | solution.py:77
  185.5 43.8 %reduce-scatter.2.cloned.1.call-done = bf16[128,2,2048]{2,0,1:T(8,128)(2,1)} async-done(((bf16[512,2,2048]{2,0,1:T(8,128)(2,1)}), bf16[128,2,2048]{2,0,1:T(8,128)(2,1)}) %reduce-scatter.2.cloned.1.call-update) | async-done | bytes 1048592 | tf_op jit(solution)/shard_map/reduce_scatter | solution.py:169
  229.3 1.8 fusion.24
  231.2 2.0 copy.64
  (28 shorter events, 0.2 us)
Async XLA Ops:
  6.5 166.3 %copy-start = (bf16[512,2048]{1,0:T(8,128)(2,1)S(1)}, bf16[512,2048]{1,0:T(8,128)(2,1)}, u32[]{:S(2)}) copy-start(bf16[512,2048]{1,0:T(8,128)(2,1)} %param.24) | copy-start | bytes 6291460
  6.5 88.7 %all-gather.3.cloned.1.call-start = ((), (), s32[]{:S(2)}) async-start(), calls=%async_computation.1 | async-start | bytes 5242880 | tf_op jit(solution)/shard_map/all_gather | solution.py:94
  8.1 41.2 %copy-start.7 = (f32[2048]{0:T(1024)S(1)}, f32[2048]{0:T(1024)}, u32[]{:S(2)}) copy-start(f32[2048]{0:T(1024)} %param.17) | copy-start | bytes 24580
  45.2 9.1 %copy-start.9 = (bf16[2048,128]{1,0:T(8,128)(2,1)S(1)}, bf16[2048,128]{1,0:T(8,128)(2,1)}, u32[]{:S(2)}) copy-start(bf16[2048,128]{1,0:T(8,128)(2,1)} %param.23) | copy-start | bytes 1572868
  45.2 9.1 %copy-start.10 = (bf16[2048,128]{1,0:T(8,128)(2,1)S(1)}, bf16[2048,128]{1,0:T(8,128)(2,1)}, u32[]{:S(2)}) copy-start(bf16[2048,128]{1,0:T(8,128)(2,1)} %param.22) | copy-start | bytes 1572868
  45.2 82.4 %all-gather.5.cloned.1.call-start = ((), (), s32[]{:S(2)}) async-start(), calls=%async_computation.2 | async-start | bytes 1310720 | tf_op jit(solution)/shard_map/all_gather | solution.py:119
  56.4 172.9 %reduce-scatter.2.cloned.1.call-start = ((), (), s32[]{:S(2)}) async-start(), calls=%async_computation.3 | async-start | bytes 5242880 | tf_op jit(solution)/shard_map/reduce_scatter | solution.py:169
  102.6 12.4 %copy-start.2 = (bf16[512,2,128]{2,0,1:T(8,128)(2,1)}, bf16[512,2,128]{2,0,1:T(8,128)(2,1)S(1)}, u32[]{:S(2)}) copy-start(bf16[512,2,128]{2,0,1:T(8,128)(2,1)S(1)} %slice.113) | copy-start | bytes 786436
  105.7 11.1 %copy-start.4 = (bf16[512,2,128]{2,0,1:T(8,128)(2,1)}, bf16[512,2,128]{2,0,1:T(8,128)(2,1)S(1)}, u32[]{:S(2)}) copy-start(bf16[512,2,128]{2,0,1:T(8,128)(2,1)S(1)} %copy.52) | copy-start | bytes 786436
  106.5 30.3 %collective-permute-start = (bf16[128,2,256]{2,0,1:T(8,128)(2,1)}, bf16[128,2,256]{2,0,1:T(8,128)(2,1)}, u32[]{:S(2)}, u32[]{:S(2)}) collective-permute-start(bf16[128,2,256]{2,0,1:T(8,128)(2,1)} %get-tuple-element.11), channel_id=1, source_target_pairs={{0,8},{8,16},{16,24},{1,9},{9,17},{17,25},{2,10},{10,18},{18,26},{... | collective-permute-start | bytes 393224 | tf_op jit(solution)/shard_map/ppermute | solution.py:22
  110.6 26.2 %collective-permute-start.1 = (bf16[128,2,256]{2,0,1:T(8,128)(2,1)}, bf16[128,2,256]{2,0,1:T(8,128)(2,1)}, u32[]{:S(2)}, u32[]{:S(2)}) collective-permute-start(bf16[128,2,256]{2,0,1:T(8,128)(2,1)} %get-tuple-element.12), channel_id=1, source_target_pairs={{8,0},{16,8},{24,16},{9,1},{17,9},{25,17},{10,2},{18,10},{26,18},{... | collective-permute-start | bytes 393224 | tf_op jit(solution)/shard_map/ppermute | solution.py:23
  127.6 9.2 %copy-start.3 = (bf16[512,2,128]{2,0,1:T(8,128)(2,1)S(1)}, bf16[512,2,128]{2,0,1:T(8,128)(2,1)}, u32[]{:S(2)}) copy-start(bf16[512,2,128]{2,0,1:T(8,128)(2,1)} %copy-done.2) | copy-start | bytes 786436
  127.6 9.2 %copy-start.5 = (bf16[512,2,128]{2,0,1:T(8,128)(2,1)S(1)}, bf16[512,2,128]{2,0,1:T(8,128)(2,1)}, u32[]{:S(2)}) copy-start(bf16[512,2,128]{2,0,1:T(8,128)(2,1)} %copy-done.4) | copy-start | bytes 786436
  137.9 6.8 %copy-start.8 = (f32[4]{0:T(128)S(1)}, f32[4]{0:T(128)}, u32[]{:S(2)}) copy-start(f32[4]{0:T(128)} %param.25) | copy-start | bytes 52
  153.3 7.4 %copy-start.6 = (bf16[1024,2,256]{2,0,1:T(8,128)(2,1)S(1)}, bf16[1024,2,256]{2,0,1:T(8,128)(2,1)}, u32[]{:S(2)}) copy-start(bf16[1024,2,256]{2,0,1:T(8,128)(2,1)} %all-gather.5.cloned.1.call-done) | copy-start | bytes 3145732
  153.3 15.6 %slice-start = ((s8[12582912]{0:T(1024)(128)(4,1)}), s8[4194304]{0:T(1024)(128)(4,1)S(1)}, s32[]{:S(2)}) async-start(s8[12582912]{0:T(1024)(128)(4,1)} %bitcast.96), calls=%async_computation.4 | async-start | bytes 8388608
  160.7 8.1 %slice-start.1 = ((s8[12582912]{0:T(1024)(128)(4,1)}), s8[4194304]{0:T(1024)(128)(4,1)S(1)}, s32[]{:S(2)}) async-start(s8[12582912]{0:T(1024)(128)(4,1)} %bitcast.96), calls=%async_computation.5 | async-start | bytes 8388608
  160.7 8.2 %slice-start.2 = ((s8[12582912]{0:T(1024)(128)(4,1)}), s8[4194304]{0:T(1024)(128)(4,1)S(1)}, s32[]{:S(2)}) async-start(s8[12582912]{0:T(1024)(128)(4,1)} %bitcast.96), calls=%async_computation.6 | async-start | bytes 8388608
  177.2 52.1 %copy-start.1 = (bf16[128,2,2048]{2,1,0:T(2,128)(2,1)S(1)}, bf16[128,2,2048]{2,1,0:T(2,128)(2,1)}, u32[]{:S(2)}) copy-start(bf16[128,2,2048]{2,1,0:T(2,128)(2,1)} %param.13) | copy-start | bytes 3145732
Sparse Core Ops, SparseCore 0:
  45.3 49.8 all-gather.2
  96.8 30.7 all-gather.4
  177.3 51.9 reduce-scatter.1
where the time goes:
time: 240 us
  waiting for transfers between devices  91.9 us (38%)
  matrix products  44.4 us (18%)
  other arithmetic  38.2 us (16%)
  blocking collectives  37.2 us (16%)
  between operations  13.4 us (6%)
  local copies, waits for them, and re-layouts  9.01 us (4%)
  starting transfers between devices  5.59 us (2%)
    reduce_scatter x1, waiting for transfers between devices, local(): lax.psum_scatter(jnp.dot(attn, w_out, preferred_element_type=jnp.float32)...  43.8 us
    all_gather x1, waiting for transfers between devices, local(): piece = lax.all_gather(hidden, 'tp', axis=0, tiled=True)  37.4 us
    psum x1, blocking collectives, local(): pair_sum, gate_sum = lax.psum((pair_part, gate_part), 'sp')  20.7 us
    all_gather x1, waiting for transfers between devices, local(): ctx_pair = lax.all_gather(local_pair, 'sp', axis=0, tiled=True)  10.6 us
    dot_general x1, matrix products, local(): jnp.einsum('qbkgd,jbkd->bkgqj', grouped, ctx_keys, preferred_element_type...  9.17 us
    reduce_sum x1, other arithmetic, local(): jnp.sum(ctx_exp, axis=-1, keepdims=True)  8.54 us
    all_gather x1, blocking collectives, local(): lax.all_gather(gate_sum, 'tp', axis=1, tiled=True)  8.28 us
    all_gather x1, blocking collectives, local(): lax.all_gather(pair_sum, 'tp', axis=2, tiled=True)  8.23 us
  transfers between devices with their start and end apart: 5, of which 3 were waited for; matrix products, arithmetic and copies ran while one was open for 16% of the time, Pallas kernels for 0%

commit v1 on v0

v1 whole, which is shorter than its diff:
```python
import functools
import math

import jax
import jax.numpy as jnp
from jax import lax
from jax.experimental import pallas as pl
from jax.experimental.pallas import tpu as pltpu
from jax.sharding import PartitionSpec as P

HEAD_DIM = 128
WINDOW = 128
GRID_W = 64
EPSILON = 1e-06
NEGATIVE = -1e30
MESH = pl.DeviceIdType.MESH
F32 = jnp.float32
BF16 = jnp.bfloat16
LOG2E = math.log2(math.e)
CHUNK = 16
SENDS = ((3, 0), (3, 1), (1, 0), (2, 1), (2, 0), (1, 1), (0, 0), (0, 1))
TARGETS = (1, 2, 1, 2, 2, 1)


def kernel(
    n_sp,
    lat_hbm,
    ctx_hbm,
    cond_ref,
    cctx_ref,
    gain_ref,
    wsh_hbm,
    wsc_hbm,
    wga_hbm,
    wq_hbm,
    wk_hbm,
    wv_hbm,
    wo_hbm,
    sink_ref,
    cos_ref,
    sin_ref,
    out_ref,
    lat_all,
    ctx_v,
    wmod,
    wqkv,
    wo,
    act_s,
    mod_p,
    mod_all,
    mod_a,
    mod_b,
    mod_g,
    hbuf,
    qbuf,
    kvbuf,
    ckv,
    abuf,
    psend,
    rs,

    loc_sem,
    modp_s,
    modp_r,
    moda_s,
    moda_r,
    lat_s,
    lat_r,
    ctx_s,
    ctx_r,
    halo_s,
    halo_r,
    rs_s,
    rs_r,
):
    samples, rows, width = lat_hbm.shape
    n_tp = mod_all.shape[0]
    wid = wmod.shape[2]
    qw = wq_hbm.shape[1]
    kw = wk_hbm.shape[1]
    heads = qw // HEAD_DIM
    lc = ctx_hbm.shape[1]
    block = rows * n_tp
    sp = lax.axis_index("sp")
    tp = lax.axis_index("tp")
    tx, ty = tp % 2, tp // 2
    peer = {1: 2 * ty + 1 - tx, 2: 2 * (1 - ty) + tx, 3: 3 - tp}

    def sp_peer(o):
        return lax.rem(sp + o, n_sp)

    loads = [
        pltpu.make_async_copy(wsh_hbm, wmod.at[0], loc_sem.at[0]),
        pltpu.make_async_copy(wsc_hbm, wmod.at[1], loc_sem.at[1]),
        pltpu.make_async_copy(wga_hbm, wmod.at[2], loc_sem.at[2]),
        pltpu.make_async_copy(ctx_hbm, ctx_v, loc_sem.at[3]),
        pltpu.make_async_copy(wk_hbm, wqkv.at[:, pl.ds(qw, kw)], loc_sem.at[4]),
        pltpu.make_async_copy(wv_hbm, wqkv.at[:, pl.ds(qw + kw, kw)], loc_sem.at[5]),
        pltpu.make_async_copy(lat_hbm, lat_all.at[0], loc_sem.at[6]),
        pltpu.make_async_copy(wq_hbm, wqkv.at[:, pl.ds(0, qw)], loc_sem.at[7]),
        pltpu.make_async_copy(wo_hbm, wo, loc_sem.at[8]),
    ]
    for load in loads:
        load.start()

    barrier = pltpu.get_barrier_semaphore()
    for o in range(1, n_sp):
        pl.semaphore_signal(barrier, inc=1, device_id={"sp": sp_peer(o)}, device_id_type=MESH)
    for k in (1, 2, 3):
        pl.semaphore_signal(barrier, inc=1, device_id={"tp": peer[k]}, device_id_type=MESH)
    pl.semaphore_wait(barrier, n_sp - 1 + n_tp - 1)

    def remote(src, dst, ssem, rsem, dev):
        return pltpu.make_async_remote_copy(
            src_ref=src, dst_ref=dst, send_sem=ssem, recv_sem=rsem, device_id=dev, device_id_type=MESH
        )

    act_s[...] = jnp.zeros_like(act_s)
    cv = cond_ref[...].astype(F32)
    act_s[0:samples, :] = cv / (1.0 + jnp.exp(-cv))
    cc = cctx_ref[...].astype(F32)
    act_s[samples : samples + 1, :] = cc / (1.0 + jnp.exp(-cc))
    both = act_s[...].astype(BF16)
    for m in range(3):
        loads[m].wait()
        mod_p[0, :, m * wid : (m + 1) * wid] = jnp.dot(both, wmod[m], preferred_element_type=F32)
    mod_copies = [
        remote(mod_p.at[0], mod_p.at[o], modp_s.at[o], modp_r.at[o], {"sp": sp_peer(o)})
        for o in range(1, n_sp)
    ]
    for copy in mod_copies:
        copy.start()

    def lat_copy(k, s, relay):
        if not relay:
            return remote(
                lat_hbm.at[s], lat_all.at[k, s], lat_s.at[k, s], lat_r.at[k, s], {"tp": peer[k]}
            )
        via, to = (1, 2) if s == 0 else (2, 1)
        return remote(
            lat_all.at[via, s], lat_all.at[3, s], lat_s.at[3, s], lat_r.at[3, s], {"tp": peer[to]}
        )

    for k, s in ((1, 0), (2, 1), (1, 1), (2, 0)):
        lat_copy(k, s, False).start()

    for copy in mod_copies:
        copy.wait_recv()
    total = mod_p[0]
    for o in range(1, n_sp):
        total = total + mod_p[o]
    mod_all[tp] = total
    all_copies = [
        remote(mod_all.at[tp], mod_all.at[tp], moda_s.at[k], moda_r.at[k], {"tp": peer[k]})
        for k in (1, 2, 3)
    ]
    for copy in all_copies:
        copy.start()
    for k in (1, 2, 3):
        remote(
            mod_all.at[peer[k]], mod_all.at[peer[k]], moda_s.at[k], moda_r.at[k], {"tp": peer[k]}
        ).wait_recv()
    for t in range(n_tp):
        cols = slice(t * wid, (t + 1) * wid)
        mod_b[:, cols] = mod_all[t, :, 0:wid]
        mod_a[:, cols] = (1.0 + mod_all[t, :, wid : 2 * wid]) * gain_ref[:, cols]
        mod_g[:, cols] = mod_all[t, :, 2 * wid : 3 * wid]

    def norm_rows(src, mod_row, base, count):
        a_row = mod_a[pl.ds(mod_row, 1), :]
        b_row = mod_b[pl.ds(mod_row, 1), :]

        @pl.loop(0, count // CHUNK)
        def _(c):
            at = pl.multiple_of(c * CHUNK, CHUNK)
            x = src[pl.ds(at, CHUNK), :].astype(F32)
            inv = lax.rsqrt(jnp.mean(x * x, axis=-1, keepdims=True) + EPSILON)
            hbuf[pl.ds(base + at, CHUNK), :] = (x * inv * a_row + b_row).astype(BF16)

    for i in (3, 4, 5):
        loads[i].wait()
    ctx_at = pl.multiple_of(sp * lc, lc)

    @pl.loop(0, samples)
    def _(s):
        norm_rows(ctx_v.at[s], samples, 0, lc)
        ckv[s, pl.ds(ctx_at, lc), :] = jnp.dot(
            hbuf[0:lc, :], wqkv[:, qw : qw + 2 * kw], preferred_element_type=F32
        ).astype(BF16)

    mine = ckv.at[:, pl.ds(ctx_at, lc), :]
    ctx_copies = [
        remote(mine, mine, ctx_s.at[o], ctx_r.at[o], {"sp": sp_peer(o)}) for o in range(1, n_sp)
    ]
    for copy in ctx_copies:
        copy.start()

    for s in (0, 1):
        lat_copy(1 if s == 0 else 2, s, False).wait_recv()
        lat_copy(3, s, True).start()

    loads[6].wait()
    loads[7].wait()
    lane = lax.broadcasted_iota(jnp.int32, (rows, HEAD_DIM), 1)
    low = lane % (HEAD_DIM // 2) < HEAD_DIM // 4

    def turn(u, cos, sin):
        other = jnp.where(
            low, pltpu.roll(u, HEAD_DIM - HEAD_DIM // 4, 1), pltpu.roll(u, HEAD_DIM // 4, 1)
        )
        return u * cos + other * sin

    @pl.loop(0, n_tp)
    def _(k):
        @pl.when(k == 1)
        def _():
            lat_copy(1, 1, False).wait_recv()

        @pl.when(k == 2)
        def _():
            lat_copy(2, 0, False).wait_recv()

        @pl.when(k == 3)
        def _():
            lat_copy(3, 0, True).wait_recv()
            lat_copy(3, 1, True).wait_recv()

        kx, ky = k % 2, k // 2
        bx = tx + kx - 2 * tx * kx
        by = ty + ky - 2 * ty * ky
        b = 2 * by + bx
        for s in range(samples):
            norm_rows(lat_all.at[k, s], s, s * rows, rows)
        at = pl.multiple_of(b * rows, rows)
        cos = cos_ref[pl.ds(at, rows), :]
        sin = sin_ref[pl.ds(at, rows), :]
        for c in range(heads // 2 + 1):
            prod = jnp.dot(
                hbuf[...], wqkv[:, c * 2 * HEAD_DIM : (c + 1) * 2 * HEAD_DIM], preferred_element_type=F32
            )
            for s in range(samples):
                part = prod[s * rows : (s + 1) * rows]
                first = turn(part[:, :HEAD_DIM], cos, sin).astype(BF16)
                if c < heads // 2:
                    second = turn(part[:, HEAD_DIM:], cos, sin).astype(BF16)
                    qbuf[s, b, 2 * c * rows : (2 * c + 1) * rows, :] = first
                    qbuf[s, b, (2 * c + 1) * rows : (2 * c + 2) * rows, :] = second
                else:
                    kvbuf[s, pl.ds(WINDOW + at, rows), 0:HEAD_DIM] = first
                    kvbuf[s, pl.ds(WINDOW + at, rows), HEAD_DIM:] = part[:, HEAD_DIM:].astype(BF16)

    halo_up = remote(
        kvbuf.at[:, pl.ds(block, WINDOW), :],
        kvbuf.at[:, pl.ds(0, WINDOW), :],
        halo_s.at[0],
        halo_r.at[0],
        {"sp": sp_peer(1)},
    )
    halo_down = remote(
        kvbuf.at[:, pl.ds(WINDOW, WINDOW), :],
        kvbuf.at[:, pl.ds(WINDOW + block, WINDOW), :],
        halo_s.at[1],
        halo_r.at[1],
        {"sp": sp_peer(n_sp - 1)},
    )
    halo_up.start()
    halo_down.start()
    loads[8].wait()
    for o in range(1, n_sp):
        got = ckv.at[:, pl.ds(pl.multiple_of(sp_peer(n_sp - o) * lc, lc), lc), :]
        remote(got, got, ctx_s.at[o], ctx_r.at[o], {"sp": sp_peer(o)}).wait_recv()
    halo_up.wait()
    halo_down.wait()

    scale = HEAD_DIM ** (-0.5) * LOG2E
    seq = block * n_sp
    nums = (((1,), (1,)), ((), ()))

    def rs_copy(i):
        return remote(
            psend.at[i], rs.at[i], rs_s.at[i], rs_r.at[i], {"tp": peer[TARGETS[i]]}
        )

    def pick(i, which):
        value = SENDS[-1][which]
        for j in range(len(SENDS) - 1):
            value = jnp.where(i == j, SENDS[j][which], value)
        return value

    span = 3 * WINDOW
    pair = 2 * rows
    row_id = lax.broadcasted_iota(jnp.int32, (pair, 1), 0)

    @pl.loop(0, 8)
    def _(i):
        k = pick(i, 0)
        s = pick(i, 1)
        kx, ky = k % 2, k // 2
        b = 2 * (ty + ky - 2 * ty * ky) + tx + kx - 2 * tx * kx
        at = pl.multiple_of(b * rows, rows)
        kc = ckv[s, :, 0:HEAD_DIM]
        vc = ckv[s, :, HEAD_DIM:]
        kl = kvbuf[s, pl.ds(at, span), 0:HEAD_DIM]
        vl = kvbuf[s, pl.ds(at, span), HEAD_DIM:]
        key = lax.broadcasted_iota(jnp.int32, (pair, span), 1)
        query = lax.broadcasted_iota(jnp.int32, (pair, span), 0) % rows
        pos = key + (sp * block + b * rows - WINDOW)
        allowed = (key >= query) & (key <= query + 2 * WINDOW) & (pos >= 0) & (pos < seq)
        for c in range(heads // 2):
            q = qbuf[s, b, c * pair : (c + 1) * pair, :]
            sc = lax.dot_general(q, kc, nums, preferred_element_type=F32)
            sl = lax.dot_general(q, kl, nums, preferred_element_type=F32)
            sl = jnp.where(allowed, sl, NEGATIVE)
            sink2 = jnp.where(row_id < rows, sink_ref[0, 2 * c], sink_ref[0, 2 * c + 1]) * LOG2E
            top = jnp.maximum(
                jnp.max(sc, axis=-1, keepdims=True), jnp.max(sl, axis=-1, keepdims=True)
            )
            top = jnp.maximum(top * scale, sink2)
            ec = jnp.exp2(sc * scale - top)
            el = jnp.exp2(sl * scale - top)
            total = (
                jnp.sum(ec, axis=-1, keepdims=True)
                + jnp.sum(el, axis=-1, keepdims=True)
                + jnp.exp2(sink2 - top)
            )
            o = jnp.dot(ec.astype(BF16), vc, preferred_element_type=F32)
            o = o + jnp.dot(el.astype(BF16), vl, preferred_element_type=F32)
            o = (o / total).astype(BF16)
            abuf[:, 2 * c * HEAD_DIM : (2 * c + 1) * HEAD_DIM] = o[:rows]
            abuf[:, (2 * c + 1) * HEAD_DIM : (2 * c + 2) * HEAD_DIM] = o[rows:]
        for n in range(n_tp):
            cols = slice(n * wid, (n + 1) * wid)
            psend[i, :, cols] = jnp.dot(
                abuf[...], wo[:, cols], preferred_element_type=F32
            ).astype(BF16)

        for j in range(4):

            @pl.when(i == j)
            def _(j=j):
                rs_copy(j).start()

        for j in (4, 5):

            @pl.when(i == j)
            def _(j=j):
                rs_copy(j - 4).wait_recv()

                @pl.loop(0, rows // CHUNK)
                def _(r):
                    part = pl.ds(pl.multiple_of(r * CHUNK, CHUNK), CHUNK)
                    psend[j, part, :] = (
                        psend[j, part, :].astype(F32) + rs[j - 4, part, :].astype(F32)
                    ).astype(BF16)

                rs_copy(j).start()

    for s in range(2):
        rs_copy(2 + s).wait_recv()
        rs_copy(4 + s).wait_recv()
        g_row = mod_g[s : s + 1, :]

        @pl.loop(0, rows // CHUNK)
        def _(r, s=s, g_row=g_row):
            part = pl.ds(pl.multiple_of(r * CHUNK, CHUNK), CHUNK)
            branch = (
                psend[6 + s, part, :].astype(F32)
                + rs[2 + s, part, :].astype(F32)
                + rs[4 + s, part, :].astype(F32)
            )
            out_ref[s, part, :] = (
                lat_all[0, s, part, :].astype(F32) + g_row * branch
            ).astype(BF16)

    for copy in mod_copies + all_copies + ctx_copies:
        copy.wait_send()
    for k, s in ((1, 0), (2, 1), (1, 1), (2, 0)):
        lat_copy(k, s, False).wait_send()
    for s in (0, 1):
        lat_copy(3, s, True).wait_send()
    for i in range(6):
        rs_copy(i).wait_send()


def local(
    n_sp,
    n_tp,
    latent,
    context,
    condition,
    ctx_condition,
    norm_gain,
    w_shift,
    w_scale,
    w_gate,
    w_query,
    w_key,
    w_value,
    w_out,
    sink,
):
    rows, samples, width = latent.shape
    lc = context.shape[0]
    wid = w_shift.shape[1]
    depth = w_shift.shape[0]
    qw, kw = w_query.shape[1], w_key.shape[1]
    heads = qw // HEAD_DIM
    block = rows * n_tp
    assert n_tp == 4 and samples == 2 and kw == HEAD_DIM and rows == WINDOW and heads % 2 == 0
    position = lax.axis_index("sp") * block + jnp.arange(block, dtype=jnp.int32)
    quarter = HEAD_DIM // 4
    lane = jnp.arange(HEAD_DIM, dtype=jnp.int32)
    freqs = 10000.0 ** (-(lane % quarter).astype(F32) / quarter)
    grid_pos = jnp.where(
        (lane < HEAD_DIM // 2)[None, :], (position // GRID_W)[:, None], (position % GRID_W)[:, None]
    ).astype(F32)
    angle = grid_pos * freqs[None, :]
    sign = jnp.where(lane % (2 * quarter) < quarter, -1.0, 1.0).astype(F32)
    cos = jnp.cos(angle)
    sin = jnp.sin(angle) * sign[None, :]
    hbm = pl.BlockSpec(memory_space=pl.ANY)
    vmem = pl.BlockSpec(memory_space=pltpu.VMEM)
    smem = pl.BlockSpec(memory_space=pltpu.SMEM)
    dma = pltpu.SemaphoreType.DMA
    mixed = pl.pallas_call(
        functools.partial(kernel, n_sp),
        out_shape=jax.ShapeDtypeStruct((samples, rows, width), BF16),
        in_specs=[hbm, hbm, vmem, vmem, vmem, hbm, hbm, hbm, hbm, hbm, hbm, hbm, smem, vmem, vmem],
        out_specs=vmem,
        scratch_shapes=[
            pltpu.VMEM((n_tp, samples, rows, width), BF16),
            pltpu.VMEM((samples, lc, width), BF16),
            pltpu.VMEM((3, depth, wid), BF16),
            pltpu.VMEM((width, qw + 2 * kw), BF16),
            pltpu.VMEM((qw, width), BF16),
            pltpu.VMEM((8, depth), F32),
            pltpu.VMEM((n_sp, 8, 3 * wid), F32),
            pltpu.VMEM((n_tp, 8, 3 * wid), F32),
            pltpu.VMEM((8, width), F32),
            pltpu.VMEM((8, width), F32),
            pltpu.VMEM((8, width), F32),
            pltpu.VMEM((max(samples * rows, lc), width), BF16),
            pltpu.VMEM((samples, n_tp, heads * rows, HEAD_DIM), BF16),
            pltpu.VMEM((samples, block + 2 * WINDOW, 2 * kw), BF16),
            pltpu.VMEM((samples, lc * n_sp, 2 * kw), BF16),
            pltpu.VMEM((rows, qw), BF16),
            pltpu.VMEM((8, rows, width), BF16),
            pltpu.VMEM((6, rows, width), BF16),
            dma((9,)),
            dma((n_sp,)),
            dma((n_sp,)),
            dma((n_tp,)),
            dma((n_tp,)),
            dma((n_tp, 2)),
            dma((n_tp, 2)),
            dma((n_sp,)),
            dma((n_sp,)),
            dma((2,)),
            dma((2,)),
            dma((6,)),
            dma((6,)),
        ],
        compiler_params=pltpu.CompilerParams(
            collective_id=0, has_side_effects=True, vmem_limit_bytes=60 * 1024 * 1024
        ),
        name="step",
    )(
        latent.transpose(1, 0, 2),
        context.transpose(1, 0, 2),
        condition,
        ctx_condition[None],
        norm_gain[None],
        w_shift,
        w_scale,
        w_gate,
        w_query,
        w_key,
        w_value,
        w_out,
        sink[None],
        cos,
        sin,
    )
    return mixed.transpose(1, 0, 2)


def solution(mesh):
    return jax.shard_map(
        functools.partial(local, mesh.shape["sp"], mesh.shape["tp"]),
        mesh=mesh,
        in_specs=(
            P(("sp", "tp"), "dp", None),
            P("sp", "dp", None),
            P("dp", "sp"),
            P("sp"),
            P(),
            P("sp", "tp"),
            P("sp", "tp"),
            P("sp", "tp"),
            P(None, "tp"),
            P(None, "tp"),
            P(None, "tp"),
            P("tp", None),
            P("tp"),
        ),
        out_specs=P(("sp", "tp"), "dp", None),
        check_vma=False,
    )
```

time: 240 us -> 117 us (0.49)
  the two profiles are of different devices: /device:TPU:0 before, /device:TPU:12 now
where the time goes in v1:
time: 117 us; the launch traced here: 116 us
  Pallas kernels  105 us (90%)
  local copies, waits for them, and re-layouts  9.45 us (8%)
  other arithmetic  1.87 us (2%)
    pallas_call x1, Pallas kernels, local(): pl.pallas_call(functools.partial(kernel, n_sp), out_shape=jax.ShapeDtypeS...  105 us
    unnamed x4, local copies, waits for them, and re-layouts  4.76 us
    transpose x1, local copies, waits for them, and re-layouts, local(): return mixed.transpose(1, 0, 2)  3.27 us

profile of v1, /device:TPU:12, one launch (start us, length us, event | category | flops | bytes accessed | tf_op | source)
XLA Modules:
  0.0 116.5 jit_solution(13408142046018984022)
XLA Ops:
  0.0 0.0 copy-start
  0.0 1.4 %broadcast_in_dim.46.cctx_ref = bf16[1,512]{1,0:T(2,128)(2,1)} reshape(bf16[512]{0:T(512)(128)(2,1)} %param.16) | data formatting | bytes 2048 | tf_op jit(solution)/shard_map/broadcast_in_dim | solution.py:471
  1.5 1.8 %sine_multiply_fusion = (f32[512,128]{1,0:T(8,128)}, f32[512,128]{1,0:T(8,128)}) fusion(f32[128]{0:T(128)S(1)} %get-tuple-element.9, f32[128]{0:T(128)S(1)} %get-tuple-element.10, s32[512]{0:T(512)S(1)} %get-tuple-element.7, s32[512]{0:T(512)S(1)} %get-tuple-element.8, pred[128]{0:T(512)(128)(4,1)S(1)} %iota_compare_fusion), kind=kLoop, calls=%fused_computation.2 | loop fusion | flops 262144 | bytes 529536 | tf_op jit(solution)/shard_map/mul | solution.py:420
  3.3 2.5 %copy.20 = bf16[128,2,2048]{2,0,1:T(8,128)(2,1)} copy(bf16[128,2,2048]{2,1,0:T(2,128)(2,1)} %param.13) | data formatting | bytes 2097152 | tf_op args[0]
  5.8 0.0 copy-done
  5.8 2.2 %copy.19 = bf16[256,2,2048]{2,0,1:T(8,128)(2,1)} copy(bf16[256,2,2048]{2,1,0:T(2,128)(2,1)S(1)} %copy-done) | data formatting | bytes 4194304 | tf_op args[1]
  8.1 105.1 %step.1 = bf16[2,128,2048]{2,1,0:T(8,128)(2,1)} custom-call(bf16[2,128,2048]{2,1,0:T(8,128)(2,1)} %bitcast.11, bf16[2,256,2048]{2,1,0:T(8,128)(2,1)} %bitcast.9, bf16[2,512]{1,0:T(2,128)(2,1)} %cond_ref.1, bf16[1,512]{1,0:T(2,128)(2,1)} %broadcast_in_dim.46.cctx_ref, f32[1,2048]{1,0:T(1,128)} %bitcast.12, bf16[512,512]{1,0:T(8,128)(2,1)} %wsh_hbm.1, ...), custom_call_target="tpu_custom_call" | custom-call | tf_op jit(solution)/shard_map/step/pallas_call | solution.py:425
  113.2 3.3 %copy.16 = bf16[128,2,2048]{2,1,0:T(2,128)(2,1)} copy(bf16[128,2,2048]{2,0,1:T(8,128)(2,1)} %bitcast.10) | data formatting | bytes 2097152 | tf_op jit(solution)/shard_map/transpose | solution.py:484
  (3 shorter events, 0.0 us)
Async XLA Ops:
  0.0 5.8 %copy-start = (bf16[256,2,2048]{2,1,0:T(2,128)(2,1)S(1)}, bf16[256,2,2048]{2,1,0:T(2,128)(2,1)}, u32[]{:S(2)}) copy-start(bf16[256,2,2048]{2,1,0:T(2,128)(2,1)} %param.14) | copy-start | bytes 6291460

commit v2 on v1

--- a/solution.py
+++ b/solution.py
@@ -37,8 +37,8 @@
     wv_hbm,
     wo_hbm,
     sink_ref,
-    cos_ref,
-    sin_ref,
+    row_ref,
+    col_ref,
     out_ref,
     lat_all,
     ctx_v,
@@ -56,6 +56,8 @@
     kvbuf,
     ckv,
     abuf,
+    cos_ref,
+    sin_ref,
     psend,
     rs,
 
@@ -66,6 +68,8 @@
     moda_r,
     lat_s,
     lat_r,
+    early_s,
+    early_r,
     ctx_s,
     ctx_r,
     halo_s,
@@ -118,7 +122,7 @@
     act_s[...] = jnp.zeros_like(act_s)
     cv = cond_ref[...].astype(F32)
     act_s[0:samples, :] = cv / (1.0 + jnp.exp(-cv))
-    cc = cctx_ref[...].astype(F32)
+    cc = cctx_ref[...].astype(F32).reshape(1, -1)
     act_s[samples : samples + 1, :] = cc / (1.0 + jnp.exp(-cc))
     both = act_s[...].astype(BF16)
     for m in range(3):
@@ -141,8 +145,23 @@
             lat_all.at[via, s], lat_all.at[3, s], lat_s.at[3, s], lat_r.at[3, s], {"tp": peer[to]}
         )
 
-    for k, s in ((1, 0), (2, 1), (1, 1), (2, 0)):
-        lat_copy(k, s, False).start()
+    half = rows // 2
+
+    def lat_part(k, s, p):
+        part = pl.ds(p * half, half)
+        return remote(
+            lat_hbm.at[s, part], lat_all.at[k, s, part], early_s.at[k, p], early_r.at[k, p], {"tp": peer[k]}
+        )
+
+    lat_part(1, 0, 0).start()
+    lat_part(2, 1, 0).start()
+
+    for which, table in ((0, cos_ref), (1, sin_ref)):
+        left = lax.broadcasted_iota(jnp.int32, (GRID_W, HEAD_DIM), 1) < HEAD_DIM // 2
+        for r in range(block // GRID_W):
+            table[r * GRID_W : (r + 1) * GRID_W, :] = jnp.where(
+                left, row_ref[which, r : r + 1, :], col_ref[which]
+            )
 
     for copy in mod_copies:
         copy.wait_recv()
@@ -156,6 +175,10 @@
     ]
     for copy in all_copies:
         copy.start()
+    lat_part(1, 0, 1).start()
+    lat_part(2, 1, 1).start()
+    lat_copy(1, 1, False).start()
+    lat_copy(2, 0, False).start()
     for k in (1, 2, 3):
         remote(
             mod_all.at[peer[k]], mod_all.at[peer[k]], moda_s.at[k], moda_r.at[k], {"tp": peer[k]}
@@ -170,7 +193,7 @@
         a_row = mod_a[pl.ds(mod_row, 1), :]
         b_row = mod_b[pl.ds(mod_row, 1), :]
 
-        @pl.loop(0, count // CHUNK)
+        @pl.loop(0, count // CHUNK, unroll=2)
         def _(c):
             at = pl.multiple_of(c * CHUNK, CHUNK)
             x = src[pl.ds(at, CHUNK), :].astype(F32)
@@ -196,7 +219,8 @@
         copy.start()
 
     for s in (0, 1):
-        lat_copy(1 if s == 0 else 2, s, False).wait_recv()
+        lat_part(1 + s, s, 0).wait_recv()
+        lat_part(1 + s, s, 1).wait_recv()
         lat_copy(3, s, True).start()
 
     loads[6].wait()
@@ -209,45 +233,6 @@
             low, pltpu.roll(u, HEAD_DIM - HEAD_DIM // 4, 1), pltpu.roll(u, HEAD_DIM // 4, 1)
         )
         return u * cos + other * sin
-
-    @pl.loop(0, n_tp)
-    def _(k):
-        @pl.when(k == 1)
-        def _():
-            lat_copy(1, 1, False).wait_recv()
-
-        @pl.when(k == 2)
-        def _():
-            lat_copy(2, 0, False).wait_recv()
-
-        @pl.when(k == 3)
-        def _():
-            lat_copy(3, 0, True).wait_recv()
-            lat_copy(3, 1, True).wait_recv()
-
-        kx, ky = k % 2, k // 2
-        bx = tx + kx - 2 * tx * kx
-        by = ty + ky - 2 * ty * ky
-        b = 2 * by + bx
-        for s in range(samples):
-            norm_rows(lat_all.at[k, s], s, s * rows, rows)
-        at = pl.multiple_of(b * rows, rows)
-        cos = cos_ref[pl.ds(at, rows), :]
-        sin = sin_ref[pl.ds(at, rows), :]
-        for c in range(heads // 2 + 1):
-            prod = jnp.dot(
-                hbuf[...], wqkv[:, c * 2 * HEAD_DIM : (c + 1) * 2 * HEAD_DIM], preferred_element_type=F32
-            )
-            for s in range(samples):
-                part = prod[s * rows : (s + 1) * rows]
-                first = turn(part[:, :HEAD_DIM], cos, sin).astype(BF16)
-                if c < heads // 2:
-                    second = turn(part[:, HEAD_DIM:], cos, sin).astype(BF16)
-                    qbuf[s, b, 2 * c * rows : (2 * c + 1) * rows, :] = first
-                    qbuf[s, b, (2 * c + 1) * rows : (2 * c + 2) * rows, :] = second
-                else:
-                    kvbuf[s, pl.ds(WINDOW + at, rows), 0:HEAD_DIM] = first
-                    kvbuf[s, pl.ds(WINDOW + at, rows), HEAD_DIM:] = part[:, HEAD_DIM:].astype(BF16)
 
     halo_up = remote(
         kvbuf.at[:, pl.ds(block, WINDOW), :],
@@ -263,14 +248,58 @@
         halo_r.at[1],
         {"sp": sp_peer(n_sp - 1)},
     )
-    halo_up.start()
-    halo_down.start()
+
+    @pl.loop(0, n_tp)
+    def _(k):
+        @pl.when(k == 1)
+        def _():
+            lat_copy(1, 1, False).wait_recv()
+
+        @pl.when(k == 2)
+        def _():
+            lat_copy(2, 0, False).wait_recv()
+
+        @pl.when(k == 3)
+        def _():
+            lat_copy(3, 0, True).wait_recv()
+            lat_copy(3, 1, True).wait_recv()
+
+        kx, ky = k % 2, k // 2
+        bx = tx + kx - 2 * tx * kx
+        by = ty + ky - 2 * ty * ky
+        b = 2 * by + bx
+        for s in range(samples):
+            norm_rows(lat_all.at[k, s], s, s * rows, rows)
+        at = pl.multiple_of(b * rows, rows)
+        cos = cos_ref[pl.ds(at, rows), :]
+        sin = sin_ref[pl.ds(at, rows), :]
+        for c in range(heads // 2 + 1):
+            prod = jnp.dot(
+                hbuf[0 : samples * rows, :], wqkv[:, c * 2 * HEAD_DIM : (c + 1) * 2 * HEAD_DIM], preferred_element_type=F32
+            )
+            for s in range(samples):
+                part = prod[s * rows : (s + 1) * rows]
+                first = turn(part[:, :HEAD_DIM], cos, sin).astype(BF16)
+                if c < heads // 2:
+                    second = turn(part[:, HEAD_DIM:], cos, sin).astype(BF16)
+                    qbuf[s, b, 2 * c * rows : (2 * c + 1) * rows, :] = first
+                    qbuf[s, b, (2 * c + 1) * rows : (2 * c + 2) * rows, :] = second
+                else:
+                    kvbuf[s, pl.ds(WINDOW + at, rows), 0:HEAD_DIM] = first
+                    kvbuf[s, pl.ds(WINDOW + at, rows), HEAD_DIM:] = part[:, HEAD_DIM:].astype(BF16)
+
+        @pl.when(b == 0)
+        def _():
+            halo_down.start()
+
+        @pl.when(b == n_tp - 1)
+        def _():
+            halo_up.start()
+
     loads[8].wait()
     for o in range(1, n_sp):
         got = ckv.at[:, pl.ds(pl.multiple_of(sp_peer(n_sp - o) * lc, lc), lc), :]
         remote(got, got, ctx_s.at[o], ctx_r.at[o], {"sp": sp_peer(o)}).wait_recv()
-    halo_up.wait()
-    halo_down.wait()
 
     scale = HEAD_DIM ** (-0.5) * LOG2E
     seq = block * n_sp
@@ -298,6 +327,16 @@
         kx, ky = k % 2, k // 2
         b = 2 * (ty + ky - 2 * ty * ky) + tx + kx - 2 * tx * kx
         at = pl.multiple_of(b * rows, rows)
+        fresh = (i == 0) | (i == 2) | (i == 3) | (i == 6)
+
+        @pl.when(fresh & (b == 0))
+        def _():
+            halo_up.wait_recv()
+
+        @pl.when(fresh & (b == n_tp - 1))
+        def _():
+            halo_down.wait_recv()
+
         kc = ckv[s, :, 0:HEAD_DIM]
         vc = ckv[s, :, HEAD_DIM:]
         kl = kvbuf[s, pl.ds(at, span), 0:HEAD_DIM]
@@ -374,10 +413,14 @@
 
     for copy in mod_copies + all_copies + ctx_copies:
         copy.wait_send()
-    for k, s in ((1, 0), (2, 1), (1, 1), (2, 0)):
+    for k, s in ((1, 1), (2, 0)):
         lat_copy(k, s, False).wait_send()
+        lat_part(k, k - 1, 0).wait_send()
+        lat_part(k, k - 1, 1).wait_send()
     for s in (0, 1):
         lat_copy(3, s, True).wait_send()
+    halo_up.wait_send()
+    halo_down.wait_send()
     for i in range(6):
         rs_copy(i).wait_send()
 
@@ -406,18 +449,20 @@
     qw, kw = w_query.shape[1], w_key.shape[1]
     heads = qw // HEAD_DIM
     block = rows * n_tp
-    assert n_tp == 4 and samples == 2 and kw == HEAD_DIM and rows == WINDOW and heads % 2 == 0
-    position = lax.axis_index("sp") * block + jnp.arange(block, dtype=jnp.int32)
+    assert n_tp == 4 and samples == 2 and kw == HEAD_DIM and rows == WINDOW and block % GRID_W == 0 and heads % 2 == 0
     quarter = HEAD_DIM // 4
     lane = jnp.arange(HEAD_DIM, dtype=jnp.int32)
     freqs = 10000.0 ** (-(lane % quarter).astype(F32) / quarter)
-    grid_pos = jnp.where(
-        (lane < HEAD_DIM // 2)[None, :], (position // GRID_W)[:, None], (position % GRID_W)[:, None]
-    ).astype(F32)
-    angle = grid_pos * freqs[None, :]
     sign = jnp.where(lane % (2 * quarter) < quarter, -1.0, 1.0).astype(F32)
-    cos = jnp.cos(angle)
-    sin = jnp.sin(angle) * sign[None, :]
+    grid_rows = block // GRID_W
+    first = lax.axis_index("sp") * grid_rows
+
+    def table(position):
+        angle = position.astype(F32)[:, None] * freqs[None, :]
+        return jnp.stack([jnp.cos(angle), jnp.sin(angle) * sign[None, :]])
+
+    row_table = table(first + jnp.arange(grid_rows, dtype=jnp.int32))
+    col_table = table(jnp.arange(GRID_W, dtype=jnp.int32))
     hbm = pl.BlockSpec(memory_space=pl.ANY)
     vmem = pl.BlockSpec(memory_space=pltpu.VMEM)
     smem = pl.BlockSpec(memory_space=pltpu.SMEM)
@@ -444,6 +489,8 @@
             pltpu.VMEM((samples, block + 2 * WINDOW, 2 * kw), BF16),
             pltpu.VMEM((samples, lc * n_sp, 2 * kw), BF16),
             pltpu.VMEM((rows, qw), BF16),
+            pltpu.VMEM((block, HEAD_DIM), F32),
+            pltpu.VMEM((block, HEAD_DIM), F32),
             pltpu.VMEM((8, rows, width), BF16),
             pltpu.VMEM((6, rows, width), BF16),
             dma((9,)),
@@ -451,6 +498,8 @@
             dma((n_sp,)),
             dma((n_tp,)),
             dma((n_tp,)),
+            dma((n_tp, 2)),
+            dma((n_tp, 2)),
             dma((n_tp, 2)),
             dma((n_tp, 2)),
             dma((n_sp,)),
@@ -468,7 +517,7 @@
         latent.transpose(1, 0, 2),
         context.transpose(1, 0, 2),
         condition,
-        ctx_condition[None],
+        ctx_condition,
         norm_gain[None],
         w_shift,
         w_scale,
@@ -478,8 +527,8 @@
         w_value,
         w_out,
         sink[None],
-        cos,
-        sin,
+        row_table,
+        col_table,
     )
     return mixed.transpose(1, 0, 2)
 

time: 117 us -> 97.8 us (0.84)
  the two profiles are of different devices: /device:TPU:12 before, /device:TPU:0 now
where the time goes in v2:
time: 97.8 us; the launch traced here: 97.6 us
  Pallas kernels  88 us (90%)
  local copies, waits for them, and re-layouts  8.03 us (8%)
  other arithmetic  1.55 us (2%)
    pallas_call x1, Pallas kernels, local(): pl.pallas_call(functools.partial(kernel, n_sp), out_shape=jax.ShapeDtypeS...  88 us
    unnamed x4, local copies, waits for them, and re-layouts  4.76 us
    transpose x1, local copies, waits for them, and re-layouts, local(): return mixed.transpose(1, 0, 2)  3.27 us

profile of v2, /device:TPU:0, one launch (start us, length us, event | category | flops | bytes accessed | tf_op | source)
XLA Modules:
  0.0 97.6 jit_solution(16613568724950367384)
XLA Ops:
  0.0 0.0 copy-start
  0.0 0.1 multiply_cosine_fusion.1
  0.1 0.6 pad_maximum_fusion.1.row_ref
  0.7 0.2 multiply_cosine_fusion
  0.9 0.6 pad_maximum_fusion.col_ref
  1.6 2.5 %copy.20 = bf16[128,2,2048]{2,0,1:T(8,128)(2,1)} copy(bf16[128,2,2048]{2,1,0:T(2,128)(2,1)} %param.13) | data formatting | bytes 2097152 | tf_op args[0]
  4.1 0.0 copy-done
  4.1 2.2 %copy.19 = bf16[256,2,2048]{2,0,1:T(8,128)(2,1)} copy(bf16[256,2,2048]{2,1,0:T(2,128)(2,1)S(1)} %copy-done) | data formatting | bytes 4194304 | tf_op args[1]
  6.3 88.0 %step.1 = bf16[2,128,2048]{2,1,0:T(8,128)(2,1)} custom-call(bf16[2,128,2048]{2,1,0:T(8,128)(2,1)} %bitcast.11, bf16[2,256,2048]{2,1,0:T(8,128)(2,1)} %bitcast.9, bf16[2,512]{1,0:T(2,128)(2,1)} %cond_ref.1, bf16[512]{0:T(512)(128)(2,1)} %cctx_ref.1, f32[1,2048]{1,0:T(1,128)} %bitcast.12, bf16[512,512]{1,0:T(8,128)(2,1)} %wsh_hbm.1, bf16[512,512]{1,0:T(8,128)(2,1)} %wsc_hbm.1, ...), custom_call_target="tpu_custom_call" | custom-call | tf_op jit(solution)/shard_map/step/pallas_call | solution.py:470
  94.3 3.3 %copy.16 = bf16[128,2,2048]{2,1,0:T(2,128)(2,1)} copy(bf16[128,2,2048]{2,0,1:T(8,128)(2,1)} %bitcast.10) | data formatting | bytes 2097152 | tf_op jit(solution)/shard_map/transpose | solution.py:533
  (3 shorter events, 0.0 us)
Async XLA Ops:
  0.0 4.1 %copy-start = (bf16[256,2,2048]{2,1,0:T(2,128)(2,1)S(1)}, bf16[256,2,2048]{2,1,0:T(2,128)(2,1)}, u32[]{:S(2)}) copy-start(bf16[256,2,2048]{2,1,0:T(2,128)(2,1)} %param.14) | copy-start | bytes 6291460

commit v3 on v2

--- a/solution.py
+++ b/solution.py
@@ -37,8 +37,10 @@
     wv_hbm,
     wo_hbm,
     sink_ref,
-    row_ref,
-    col_ref,
+    row_cos,
+    row_sin,
+    col_cos,
+    col_sin,
     out_ref,
     lat_all,
     ctx_v,
@@ -156,11 +158,11 @@
     lat_part(1, 0, 0).start()
     lat_part(2, 1, 0).start()
 
-    for which, table in ((0, cos_ref), (1, sin_ref)):
+    for by_row, by_col, table in ((row_cos, col_cos, cos_ref), (row_sin, col_sin, sin_ref)):
         left = lax.broadcasted_iota(jnp.int32, (GRID_W, HEAD_DIM), 1) < HEAD_DIM // 2
         for r in range(block // GRID_W):
             table[r * GRID_W : (r + 1) * GRID_W, :] = jnp.where(
-                left, row_ref[which, r : r + 1, :], col_ref[which]
+                left, by_row[r : r + 1, :], by_col[...]
             )
 
     for copy in mod_copies:
@@ -193,7 +195,7 @@
         a_row = mod_a[pl.ds(mod_row, 1), :]
         b_row = mod_b[pl.ds(mod_row, 1), :]
 
-        @pl.loop(0, count // CHUNK, unroll=2)
+        @pl.loop(0, count // CHUNK, unroll=4)
         def _(c):
             at = pl.multiple_of(c * CHUNK, CHUNK)
             x = src[pl.ds(at, CHUNK), :].astype(F32)
@@ -399,7 +401,7 @@
         rs_copy(4 + s).wait_recv()
         g_row = mod_g[s : s + 1, :]
 
-        @pl.loop(0, rows // CHUNK)
+        @pl.loop(0, rows // CHUNK, unroll=2)
         def _(r, s=s, g_row=g_row):
             part = pl.ds(pl.multiple_of(r * CHUNK, CHUNK), CHUNK)
             branch = (
@@ -459,7 +461,7 @@
 
     def table(position):
         angle = position.astype(F32)[:, None] * freqs[None, :]
-        return jnp.stack([jnp.cos(angle), jnp.sin(angle) * sign[None, :]])
+        return jnp.cos(angle), jnp.sin(angle) * sign[None, :]
 
     row_table = table(first + jnp.arange(grid_rows, dtype=jnp.int32))
     col_table = table(jnp.arange(GRID_W, dtype=jnp.int32))
@@ -470,7 +472,7 @@
     mixed = pl.pallas_call(
         functools.partial(kernel, n_sp),
         out_shape=jax.ShapeDtypeStruct((samples, rows, width), BF16),
-        in_specs=[hbm, hbm, vmem, vmem, vmem, hbm, hbm, hbm, hbm, hbm, hbm, hbm, smem, vmem, vmem],
+        in_specs=[hbm, hbm, vmem, vmem, vmem, hbm, hbm, hbm, hbm, hbm, hbm, hbm, smem, vmem, vmem, vmem, vmem],
         out_specs=vmem,
         scratch_shapes=[
             pltpu.VMEM((n_tp, samples, rows, width), BF16),
@@ -527,8 +529,8 @@
         w_value,
         w_out,
         sink[None],
-        row_table,
-        col_table,
+        *row_table,
+        *col_table,
     )
     return mixed.transpose(1, 0, 2)
 

time: 97.8 us -> 97.3 us (level)
    mul x0 -> x2, other arithmetic: none -> 1.53 us  [table(): return (jnp.cos(angle), jnp.sin(angle) * sign[None, :])]
    another operation x2 -> x0, other arithmetic: 1.23 us -> none  [table(): return jnp.stack([jnp.cos(angle), jnp.sin(angle) * sign[None, :]])]
where the time goes in v3:
time: 97.3 us; the launch traced here: 97.1 us
  Pallas kernels  87.5 us (90%)
  local copies, waits for them, and re-layouts  8.03 us (8%)
  other arithmetic  1.54 us (2%)
    pallas_call x1, Pallas kernels, local(): pl.pallas_call(functools.partial(kernel, n_sp), out_shape=jax.ShapeDtypeS...  87.5 us
    unnamed x4, local copies, waits for them, and re-layouts  4.76 us
    transpose x1, local copies, waits for them, and re-layouts, local(): return mixed.transpose(1, 0, 2)  3.27 us

profile of v3, /device:TPU:0, one launch (start us, length us, event | category | flops | bytes accessed | tf_op | source)
XLA Modules:
  0.0 97.1 jit_solution(4480815051383462764)
XLA Ops:
  0.0 0.0 copy-start
  0.0 0.7 fusion.1
  0.7 0.8 fusion
  1.5 2.5 %copy.20 = bf16[128,2,2048]{2,0,1:T(8,128)(2,1)} copy(bf16[128,2,2048]{2,1,0:T(2,128)(2,1)} %param.13) | data formatting | bytes 2097152 | tf_op args[0]
  4.1 0.0 copy-done
  4.1 2.2 %copy.19 = bf16[256,2,2048]{2,0,1:T(8,128)(2,1)} copy(bf16[256,2,2048]{2,1,0:T(2,128)(2,1)S(1)} %copy-done) | data formatting | bytes 4194304 | tf_op args[1]
  6.3 87.5 %step.1 = bf16[2,128,2048]{2,1,0:T(8,128)(2,1)} custom-call(bf16[2,128,2048]{2,1,0:T(8,128)(2,1)} %bitcast.11, bf16[2,256,2048]{2,1,0:T(8,128)(2,1)} %bitcast.9, bf16[2,512]{1,0:T(2,128)(2,1)} %cond_ref.1, bf16[512]{0:T(512)(128)(2,1)} %cctx_ref.1, f32[1,2048]{1,0:T(1,128)} %bitcast.12, bf16[512,512]{1,0:T(8,128)(2,1)} %wsh_hbm.1, bf16[512,512]{1,0:T(8,128)(2,1)} %wsc_hbm.1, ...), custom_call_target="tpu_custom_call" | custom-call | tf_op jit(solution)/shard_map/step/pallas_call | solution.py:472
  93.8 3.3 %copy.16 = bf16[128,2,2048]{2,1,0:T(2,128)(2,1)} copy(bf16[128,2,2048]{2,0,1:T(8,128)(2,1)} %bitcast.10) | data formatting | bytes 2097152 | tf_op jit(solution)/shard_map/transpose | solution.py:535
  (3 shorter events, 0.0 us)
Async XLA Ops:
  0.0 4.1 %copy-start = (bf16[256,2,2048]{2,1,0:T(2,128)(2,1)S(1)}, bf16[256,2,2048]{2,1,0:T(2,128)(2,1)}, u32[]{:S(2)}) copy-start(bf16[256,2,2048]{2,1,0:T(2,128)(2,1)} %param.14) | copy-start | bytes 6291460
